TPU v7x, 32 devices: a whole 2x2x4 slice. The times are simulated.
32 devices in a mesh: sp: 16 (over z, y, x), tp: 2 (over core).
Axes of the slice: x: 2, y: 2, z: 4, core: 2. Of those that a mesh axis runs over, the one named last changes fastest.
Arguments:
- normed: bfloat16 [4096, 2048], P(('sp', 'tp')), may hold values from -40 to 40
- query_weight: bfloat16 [2048, 2048], P(None, 'tp'), may hold values from -1.5 to 1.5
- key_weight: bfloat16 [2048, 2048], P(None, 'tp'), may hold values from -1 to 1
- value_weight: bfloat16 [2048, 2048], P(None, 'tp'), may hold values from -0.125 to 0.125
- pool_in_weight: bfloat16 [2048, 1024], P(None, 'tp'), may hold values from -0.125 to 0.125
- pool_weight: bfloat16 [8, 128, 128], P('tp'), may hold values from -0.5 to 0.5
- map_balance: float32 [8], replicated, may hold values from 0.3 to 0.8
- head_gain: float32 [256], replicated, may hold values from 0.1 to 1.9
- contrast_out_weight: bfloat16 [2048, 2048], P('tp'), may hold values from -0.109375 to 0.109375
- pool_out_weight: bfloat16 [1024, 2048], P('tp'), may hold values from -0.109375 to 0.109375
Outputs:
- layer_out: bfloat16 [4096, 2048], P(('sp', 'tp'))
All inputs are finite; a program needn't handle non-finite values.
Results may differ from a plain program's by a relative error of at most 0.03.
Values may be sent and summed in bfloat16 or wider, within the bound.
A program may use at most 128 MiB of HBM per device.

v0:
```python
import math

import jax
import jax.numpy as jnp
from jax import lax
from jax.sharding import PartitionSpec as P

reach_back = 15
norm_epsilon = 1e-06


def passed_along(block, axis, distance):
    devices = range(lax.axis_size(axis))
    route = [(i - distance, i) for i in devices if i - distance in devices]
    return lax.ppermute(block, axis, route)


def from_partner(block, axis, stride):
    count = lax.axis_size(axis)
    route = []
    for low in range(count):
        high = low | 1 << stride
        if high != low and high < count:
            route += [(low, high), (high, low)]
    return lax.ppermute(block, axis, route)


def shifted(array, axis, by):
    size = lax.axis_size(axis)
    return lax.ppermute(array, axis, [(i, (i + by) % size) for i in range(size)])


def as_sent(array):

    def short(part):
        return part.astype(jnp.bfloat16) if part.dtype == jnp.float32 else part

    return jax.tree.map(short, array)


def attend(running, queries, key_rows, value_rows, query_first, key_first, score_scale):
    key_count = key_rows.shape[0]
    key_block = math.gcd(key_count, 1024)
    unit_count = queries.shape[1]
    heads_here = value_rows.shape[1]
    per_head = unit_count // heads_here
    query_count = queries.shape[0]
    query_order = query_first + lax.iota(jnp.int32, query_count)

    def key_step(block_index, carried):
        block_start = block_index * key_block

        def block_work(current):
            row_peak, row_total, weighted = current
            scores = (
                jnp.einsum("qud,kud->uqk", queries, key_rows, preferred_element_type=jnp.float32)
                * score_scale
            )
            key_order = key_first + block_start + lax.iota(jnp.int32, key_block)
            scores = jnp.where(
                key_order[None, None, :] <= query_order[None, :, None], scores, -jnp.inf
            )
            new_peak = jnp.maximum(row_peak, jnp.max(scores, axis=2))
            shrink = jnp.exp(row_peak - new_peak)
            raised = jnp.exp(scores - new_peak[:, :, None])
            row_total = row_total * shrink + jnp.sum(raised, axis=2)
            map_weights = raised.astype(jnp.bfloat16).reshape(
                heads_here, per_head, query_count, key_block
            )
            update = jnp.einsum(
                "hmqk,khe->hmqe", map_weights, value_rows, preferred_element_type=jnp.float32
            )
            weighted = weighted * shrink[:, :, None] + update.reshape(unit_count, query_count, -1)
            return (new_peak, row_total, weighted)

        def keep_state(current):
            return current

        return lax.cond(
            key_first + block_start <= query_first + query_count - 1,
            block_work,
            keep_state,
            carried,
        )

    return lax.fori_loop(0, key_count // key_block, key_step, running)


def fresh_state(unit_count, row_count, value_width):
    return (
        jnp.full((unit_count, row_count), -1e30, jnp.float32),
        jnp.zeros((unit_count, row_count), jnp.float32),
        jnp.zeros((unit_count, row_count, value_width), jnp.float32),
    )


def finished(running):
    row_peak, row_total, weighted = running
    return (weighted / row_total[:, :, None]).astype(jnp.bfloat16)


def joined_state(first, second):
    first_peak, first_total, first_weighted = first
    second_peak, second_total, second_weighted = second
    new_peak = jnp.maximum(first_peak, second_peak)
    first_shrink = jnp.exp(first_peak - new_peak)
    second_shrink = jnp.exp(second_peak - new_peak)
    new_total = first_total * first_shrink + second_total * second_shrink
    new_weighted = (
        first_weighted * first_shrink[:, :, None] + second_weighted * second_shrink[:, :, None]
    )
    return (new_peak, new_total, new_weighted)


def per_device(
    normed,
    query_weight,
    key_weight,
    value_weight,
    pool_in_weight,
    pool_weight,
    map_balance,
    head_gain,
    contrast_out_weight,
    pool_out_weight,
):
    tp_index = lax.axis_index("tp")
    sp_count = lax.axis_size("sp")
    sp_index = lax.axis_index("sp")
    head_dim = head_gain.shape[0] // 2
    value_width = 2 * head_dim
    query_cols = query_weight.shape[1]
    value_cols = value_weight.shape[1]
    unit_count = query_cols // head_dim
    heads_here = unit_count // 2
    project_incoming = lax.all_gather(normed, "tp", axis=0, tiled=True)
    products = [
        jnp.dot(project_incoming, weight_part, preferred_element_type=jnp.float32)
        for weight_part in (query_weight, key_weight, value_weight, pool_in_weight)
    ]
    joined = jnp.concatenate(products, axis=1).astype(jnp.bfloat16)
    row_count = joined.shape[0]
    queries = joined[:, :query_cols].reshape(row_count, unit_count, head_dim)
    key_rows = joined[:, query_cols : 2 * query_cols].reshape(row_count, unit_count, head_dim)
    value_rows = joined[:, 2 * query_cols : 2 * query_cols + value_cols].reshape(
        row_count, heads_here, value_width
    )
    pool_input = joined[:, 2 * query_cols + value_cols :]
    pool_cols = pool_input.shape[1]
    upper_rim = passed_along(pool_input[row_count - reach_back :], "sp", 1)
    extended = jnp.concatenate([upper_rim, pool_input], axis=0).astype(jnp.float32)
    groups_here = pool_weight.shape[0]
    group_width = pool_weight.shape[1]
    group_index = tp_index * groups_here + lax.iota(jnp.int32, pool_cols) // group_width
    widths = jnp.left_shift(jnp.int32(2), group_index % 4)
    window_sum = jnp.zeros((row_count, pool_cols), jnp.float32)
    for offset in range(reach_back + 1):
        window_sum = window_sum + extended[
            reach_back - offset : reach_back - offset + row_count
        ] * (offset < widths)[None, :].astype(jnp.float32)
    position = sp_index * row_count + lax.iota(jnp.int32, row_count)
    counts = jnp.minimum(position[:, None] + 1, widths[None, :]).astype(jnp.float32)
    spread = (window_sum / counts - extended[reach_back:]).astype(jnp.bfloat16)
    mixed_groups = jnp.einsum(
        "tgc,gce->tge",
        spread.reshape(row_count, groups_here, group_width),
        pool_weight,
        preferred_element_type=jnp.float32,
    )
    pool_out = mixed_groups.reshape(row_count, pool_cols).astype(jnp.bfloat16)
    score_scale = head_dim ** (-0.5)
    level_count = sp_count.bit_length() - 1
    low_levels = level_count // 2
    band_size = 1 << low_levels
    band_count = sp_count // band_size
    member = sp_index % band_size
    band = sp_index // band_size
    band_queries = queries
    for bit in range(low_levels):
        received = from_partner(band_queries, "sp", bit)
        upper = member >> bit & 1 == 1
        band_queries = jnp.where(
            upper,
            jnp.concatenate([received, band_queries], axis=0),
            jnp.concatenate([band_queries, received], axis=0),
        )
    band_first = band * band_size * row_count
    running = fresh_state(unit_count, band_size * row_count, value_width)
    for step in range(band_count):
        if step == 0:
            key_piece, value_piece = (key_rows, value_rows)
        else:
            key_piece, value_piece = shifted((key_rows, value_rows), "sp", step * band_size)
        source = (sp_index - step * band_size) % sp_count
        running = attend(
            running,
            band_queries,
            key_piece,
            value_piece,
            band_first,
            source * row_count,
            score_scale,
        )
    for bit in range(low_levels - 1, -1, -1):
        half = running[0].shape[1] // 2
        upper = member >> bit & 1 == 1
        lower_part = jax.tree.map(lambda item: item[:, :half], running)
        upper_part = jax.tree.map(lambda item: item[:, half:], running)
        outgoing = jax.tree.map(
            lambda low, high: jnp.where(upper, low, high), lower_part, upper_part
        )
        kept = jax.tree.map(lambda low, high: jnp.where(upper, high, low), lower_part, upper_part)
        incoming = from_partner(
            (as_sent(outgoing[0]), as_sent(outgoing[1]), as_sent(outgoing[2])), "sp", bit
        )
        running = joined_state(kept, incoming)
    maps = finished(running)
    paired = maps.reshape(heads_here, 2, row_count, value_width)
    paired = lax.optimization_barrier(paired).astype(jnp.float32)
    head_first = tp_index * heads_here
    balance_here = lax.dynamic_slice_in_dim(map_balance, head_first, heads_here, 0)
    contrast = paired[:, 0] - balance_here[:, None, None] * paired[:, 1]
    mean_square = jnp.mean(contrast * contrast, axis=2, keepdims=True)
    contrast = contrast * lax.rsqrt(mean_square + norm_epsilon) * head_gain
    contrast_out = (
        contrast.astype(jnp.bfloat16)
        .transpose(1, 0, 2)
        .reshape(row_count, heads_here * value_width)
    )
    partial_value = jnp.dot(contrast_out, contrast_out_weight, preferred_element_type=jnp.float32)
    return lax.psum_scatter(
        (
            partial_value + jnp.dot(pool_out, pool_out_weight, preferred_element_type=jnp.float32)
        ).astype(jnp.bfloat16),
        "tp",
        scatter_dimension=0,
        tiled=True,
    )


def solution(mesh):
    return jax.shard_map(
        per_device,
        mesh=mesh,
        in_specs=(
            P(("sp", "tp"), None),
            P(None, "tp"),
            P(None, "tp"),
            P(None, "tp"),
            P(None, "tp"),
            P("tp", None, None),
            P(),
            P(),
            P("tp", None),
            P("tp", None),
        ),
        out_specs=P(("sp", "tp"), None),
        check_vma=False,
    )
```

profile of v0, /device:TPU:25, one launch (start us, length us, event | category | flops | bytes accessed | tf_op | source)
XLA Modules:
  0.0 269.3 jit_solution(1094205833064472675)
XLA Ops:
  6.5 0.7 all-gather.2.cloned.1.call-update
  7.3 12.3 %all-gather.2.cloned.1.call-done = bf16[256,2048]{1,0:T(8,128)(2,1)} async-done(((bf16[128,2048]{1,0:T(8,128)(2,1)}), bf16[256,2048]{1,0:T(8,128)(2,1)}) %all-gather.2.cloned.1.call-update) | async-done | bytes 1048592 | tf_op jit(solution)/shard_map/all_gather | solution.py:136
  19.6 3.8 %fusion.23 = bf16[32,8,8,128]{3,2,1,0:T(8,128)(2,1)S(1)} fusion(bf16[256,2048]{1,0:T(8,128)(2,1)} %all-gather.2.cloned.1.call-done, bf16[2048,1024]{1,0:T(8,128)(2,1)} %param.19), kind=kOutput, calls=%fused_computation.60 | convolution fusion | flops 1074003968 | bytes 5767168 | tf_op jit(solution)/shard_map/dot_general | solution.py:138
  23.5 1.3 collective-permute-start
  24.8 12.2 %collective-permute-done = bf16[256,8,128]{2,0,1:T(8,128)(2,1)} collective-permute-done((bf16[256,8,128]{2,0,1:T(8,128)(2,1)S(1)}, bf16[256,8,128]{2,0,1:T(8,128)(2,1)}, u32[]{:S(2)}, u32[]{:S(2)}) %collective-permute-start) | collective-permute-done | bytes 524320 | tf_op jit(solution)/shard_map/ppermute | solution.py:25
  37.0 1.9 maximum_select_fusion.1
  38.9 1.3 collective-permute-start.1
  40.1 4.0 %convolution_convert_fusion.1 = bf16[256,1024]{1,0:T(8,128)(2,1)S(1)} fusion(bf16[256,2048]{1,0:T(8,128)(2,1)} %all-gather.2.cloned.1.call-done, bf16[2048,1024]{1,0:T(8,128)(2,1)} %param.20), kind=kOutput, calls=%fused_computation.58 | convolution fusion | flops 1074003968 | bytes 5767168 | tf_op jit(solution)/shard_map/dot_general | solution.py:138
  44.2 1.0 copy_bitcast_fusion.1
  45.2 1.3 convolution_convert_fusion
  46.5 0.9 copy.95
  47.3 1.4 collective-permute-start.3
  48.8 1.2 collective-permute-start.4
  50.0 1.1 collective-permute-start.5
  51.1 6.6 %collective-permute-done.2 = bf16[256,8,128]{2,0,1:T(8,128)(2,1)S(1)} collective-permute-done((bf16[256,8,128]{2,0,1:T(8,128)(2,1)}, bf16[256,8,128]{2,0,1:T(8,128)(2,1)S(1)}, u32[]{:S(2)}, u32[]{:S(2)}) %collective-permute-start.2) | collective-permute-done | bytes 524320 | tf_op jit(solution)/shard_map/ppermute | solution.py:30
  57.8 0.3 collective-permute-start.6
  58.0 4.7 %collective-permute-done.1 = bf16[512,8,128]{2,0,1:T(8,128)(2,1)S(1)} collective-permute-done((bf16[512,8,128]{2,0,1:T(8,128)(2,1)S(1)}, bf16[512,8,128]{2,0,1:T(8,128)(2,1)S(1)}, u32[]{:S(2)}, u32[]{:S(2)}) %collective-permute-start.1) | collective-permute-done | bytes 1048608 | tf_op jit(solution)/shard_map/ppermute | solution.py:25
  62.7 1.0 copy-done.5
  63.7 0.3 collective-permute-start.7
  64.0 4.0 %broadcast_in_dim.65 = f32[8,1024,256]{2,1,0:T(8,128)} broadcast(f32[]{:T(128)} %constant.213.clone.1), dimensions={} | broadcast | bytes 8388612 | tf_op jit(solution)/shard_map/broadcast_in_dim | solution.py:93
  68.1 2.2 reshape.326
  70.3 1.9 copy.81
  72.2 3.5 %maximum_select_fusion = bf16[1024,8,128]{2,0,1:T(8,128)(2,1)} fusion(bf16[512,8,128]{2,0,1:T(8,128)(2,1)S(1)} %maximum_select_fusion.1, bf16[512,8,128]{2,0,1:T(8,128)(2,1)} %copy-done.5, pred[]{:T(512)S(6)} %eq.17), kind=kLoop, calls=%fused_computation.54 | loop fusion | flops 9437184 | bytes 4194305 | tf_op jit(solution)/shard_map/jit(_where)/select_n | solution.py:182
  75.7 13.8 %conditional.4 = ((f32[8,1024]{1,0:T(8,128)S(1)}, f32[8,1024]{1,0:T(8,128)S(1)}, f32[8,1024,256]{2,1,0:T(8,128)})) conditional(s32[]{:T(128)} %convert_element_type.230, (f32[8,1024]{1,0:T(8,128)S(1)}, f32[8,1024]{1,0:T(8,128)S(1)}, f32[8,1024,256]{2,1,0:T(8,128)}) %tuple.64, (s32[]{:T(128)}, s32[1024]{0:T(1024)S(1)}, ...), branch_computations={%region_0.1_spmd, %region_1.4_spmd} | conditional | flops 1631863040 | bytes 65247296 | solution.py:79
  76.0 3.2 %fusion = (f32[8,1024]{1,0:T(8,128)S(1)}, f32[8,1024,256]{1,2,0:T(8,128)S(1)}) fusion(pred[1024,256]{0,1:T(8,128)(4,1)S(1)} %broadcast_compare_fusion, bf16[1024,8,128]{2,0,1:T(8,128)(2,1)} %get-tuple-element.304, bf16[256,8,128]{2,1,0:T(8,128)(2,1)} %get-tuple-element.408), kind=kOutput, calls=%fused_computation.3 | convolution fusion | flops 543154176 | bytes 11304960 | tf_op jit(solution)/shard_map/while/body/eval_jaxpr/cond/branch_1_fun/qud,kud->uqk/dot_general | solution.py:56
  79.2 2.0 fusion.1
  81.3 1.8 fusion.3
  83.1 6.4 %bitcast_add_fusion = f32[8,1024,256]{2,1,0:T(8,128)} fusion(f32[4,2,1024,256]{3,2,1,0:T(8,128)S(1)} %fusion.3, f32[8,1024,256]{2,1,0:T(8,128)} %get-tuple-element.307, f32[8,1024]{1,0:T(8,128)S(1)} %get-tuple-element.417), kind=kLoop, calls=%fused_computation | loop fusion | flops 4194304 | bytes 25198592 | tf_op jit(solution)/shard_map/while/body/eval_jaxpr/cond/branch_1_fun/add | solution.py:73
  89.5 14.8 %conditional.5 = ((f32[8,1024]{1,0:T(8,128)S(1)}, f32[8,1024]{1,0:T(8,128)S(1)}, f32[8,1024,256]{2,1,0:T(8,128)})) conditional(s32[]{:T(128)} %convert_element_type.229, (f32[8,1024]{1,0:T(8,128)S(1)}, f32[8,1024]{1,0:T(8,128)S(1)}, f32[8,1024,256]{2,1,0:T(8,128)}) %get-tuple-element.487, (s32[]{:T(128)}, s32[1024]{0:T(1024)S(1)}, ...), branch_computations={%region_4.5_spmd, %region_5.8_spmd} | conditional | flops 1631863040 | bytes 63150116 | solution.py:79
  90.0 3.0 %fusion.7 = (f32[8,1024]{1,0:T(8,128)S(1)}, f32[8,1024,256]{1,2,0:T(8,128)S(1)}) fusion(pred[1024,256]{0,1:T(8,128)(4,1)S(1)} %broadcast_compare_fusion.1, bf16[1024,8,128]{2,0,1:T(8,128)(2,1)} %get-tuple-element.312, bf16[256,8,128]{2,0,1:T(8,128)(2,1)S(1)} %get-tuple-element.313), kind=kOutput, calls=%fused_computation.17 | convolution fusion | flops 543154176 | bytes 11304960 | tf_op jit(solution)/shard_map/while/body/eval_jaxpr/cond/branch_1_fun/qud,kud->uqk/dot_general | solution.py:56
  93.0 2.0 fusion.8
  95.1 2.8 %fusion.10 = f32[4,2,1024,256]{3,2,1,0:T(8,128)S(1)} fusion(bf16[4,2,1024,256]{2,3,1,0:T(8,128)(2,1)S(1)} %bitcast.103, bf16[256,4,256]{2,0,1:T(8,128)(2,1)} %get-tuple-element.316), kind=kOutput, calls=%fused_computation.20 | convolution fusion | flops 1073741824 | bytes 13107200 | tf_op jit(solution)/shard_map/while/body/eval_jaxpr/cond/branch_1_fun/hmqk,khe->hmqe/dot_general | solution.py:70
  97.9 6.4 %bitcast_add_fusion.1 = f32[8,1024,256]{2,1,0:T(8,128)} fusion(f32[4,2,1024,256]{3,2,1,0:T(8,128)S(1)} %fusion.10, f32[8,1024,256]{2,1,0:T(8,128)} %get-tuple-element.315, f32[8,1024]{1,0:T(8,128)S(1)} %get-tuple-element.419), kind=kLoop, calls=%fused_computation.14 | loop fusion | flops 4194304 | bytes 25198592 | tf_op jit(solution)/shard_map/while/body/eval_jaxpr/cond/branch_1_fun/add | solution.py:73
  104.4 20.9 %collective-permute-done.4 = bf16[256,8,128]{2,0,1:T(8,128)(2,1)} collective-permute-done((bf16[256,8,128]{2,0,1:T(8,128)(2,1)}, bf16[256,8,128]{2,0,1:T(8,128)(2,1)}, u32[]{:S(2)}, u32[]{:S(2)}) %collective-permute-start.4) | collective-permute-done | bytes 524320 | tf_op jit(solution)/shard_map/ppermute | solution.py:30
  125.2 11.2 %collective-permute-done.5 = bf16[256,4,256]{2,0,1:T(8,128)(2,1)} collective-permute-done((bf16[256,4,256]{2,0,1:T(8,128)(2,1)}, bf16[256,4,256]{2,0,1:T(8,128)(2,1)}, u32[]{:S(2)}, u32[]{:S(2)}) %collective-permute-start.5) | collective-permute-done | bytes 524320 | tf_op jit(solution)/shard_map/ppermute | solution.py:30
  136.5 14.7 %conditional.6 = ((f32[8,1024]{1,0:T(8,128)S(1)}, f32[8,1024]{1,0:T(8,128)S(1)}, f32[8,1024,256]{2,1,0:T(8,128)})) conditional(s32[]{:T(128)} %convert_element_type.228, (f32[8,1024]{1,0:T(8,128)S(1)}, f32[8,1024]{1,0:T(8,128)S(1)}, f32[8,1024,256]{2,1,0:T(8,128)}) %get-tuple-element.488, (s32[]{:T(128)}, s32[1024]{0:T(1024)S(1)}, ...), branch_computations={%region_8.9_spmd, %region_9.12_spmd} | conditional | flops 1631863040 | bytes 63150116 | solution.py:79
  136.5 0.2 broadcast_compare_fusion.2
  136.7 3.1 %fusion.12 = (f32[8,1024]{1,0:T(8,128)S(1)}, f32[8,1024,256]{1,2,0:T(8,128)S(1)}) fusion(pred[1024,256]{0,1:T(8,128)(4,1)S(1)} %broadcast_compare_fusion.2, bf16[1024,8,128]{2,0,1:T(8,128)(2,1)} %get-tuple-element.320, bf16[256,8,128]{2,0,1:T(8,128)(2,1)} %get-tuple-element.321), kind=kOutput, calls=%fused_computation.29 | convolution fusion | flops 543154176 | bytes 11304960 | tf_op jit(solution)/shard_map/while/body/eval_jaxpr/cond/branch_1_fun/qud,kud->uqk/dot_general | solution.py:56
  139.8 2.0 fusion.13
  141.9 2.8 %fusion.15 = f32[4,2,1024,256]{3,2,1,0:T(8,128)S(1)} fusion(bf16[4,2,1024,256]{2,3,1,0:T(8,128)(2,1)S(1)} %bitcast.104, bf16[256,4,256]{2,0,1:T(8,128)(2,1)} %get-tuple-element.324), kind=kOutput, calls=%fused_computation.32 | convolution fusion | flops 1073741824 | bytes 13107200 | tf_op jit(solution)/shard_map/while/body/eval_jaxpr/cond/branch_1_fun/hmqk,khe->hmqe/dot_general | solution.py:70
  144.7 6.4 %bitcast_add_fusion.2 = f32[8,1024,256]{2,1,0:T(8,128)} fusion(f32[4,2,1024,256]{3,2,1,0:T(8,128)S(1)} %fusion.15, f32[8,1024,256]{2,1,0:T(8,128)} %get-tuple-element.323, f32[8,1024]{1,0:T(8,128)S(1)} %get-tuple-element.421), kind=kLoop, calls=%fused_computation.26 | loop fusion | flops 4194304 | bytes 25198592 | tf_op jit(solution)/shard_map/while/body/eval_jaxpr/cond/branch_1_fun/add | solution.py:73
  151.2 14.9 %conditional.7 = (f32[8,1024,256]{2,1,0:T(8,128)}, f32[8,1024]{1,0:T(8,128)S(1)}, f32[8,1024]{1,0:T(8,128)S(1)}) conditional(s32[]{:T(128)} %convert_element_type.227, (f32[8,1024]{1,0:T(8,128)S(1)}, f32[8,1024]{1,0:T(8,128)S(1)}, f32[8,1024,256]{2,1,0:T(8,128)}) %get-tuple-element.489, (s32[]{:T(128)}, s32[1024]{0:T(1024)S(1)}, ...), branch_computations={%region_12.13_spmd.clone, %region_13.16_spmd.clone} | conditional | flops 1631863040 | bytes 63150108 | solution.py:79
  151.7 3.1 %fusion.17 = (f32[8,1024]{1,0:T(8,128)S(1)}, f32[8,1024,256]{1,2,0:T(8,128)S(1)}) fusion(pred[1024,256]{0,1:T(8,128)(4,1)S(1)} %broadcast_compare_fusion.3, bf16[1024,8,128]{2,0,1:T(8,128)(2,1)} %get-tuple-element.378, bf16[256,8,128]{2,0,1:T(8,128)(2,1)} %get-tuple-element.379), kind=kOutput, calls=%fused_computation.41 | convolution fusion | flops 543154176 | bytes 11304960 | tf_op jit(solution)/shard_map/while/body/eval_jaxpr/cond/branch_1_fun/qud,kud->uqk/dot_general | solution.py:56
  154.8 2.0 fusion.19
  156.8 2.8 %fusion.20 = f32[4,2,1024,256]{3,2,1,0:T(8,128)S(1)} fusion(bf16[4,2,1024,256]{2,3,1,0:T(8,128)(2,1)S(1)} %bitcast.105, bf16[256,4,256]{2,0,1:T(8,128)(2,1)} %get-tuple-element.382), kind=kOutput, calls=%fused_computation.44 | convolution fusion | flops 1073741824 | bytes 13107200 | tf_op jit(solution)/shard_map/while/body/eval_jaxpr/cond/branch_1_fun/hmqk,khe->hmqe/dot_general | solution.py:70
  159.7 6.4 %bitcast_add_fusion.3 = f32[8,1024,256]{2,1,0:T(8,128)} fusion(f32[4,2,1024,256]{3,2,1,0:T(8,128)S(1)} %fusion.20, f32[8,1024,256]{2,1,0:T(8,128)} %get-tuple-element.381, f32[8,1024]{1,0:T(8,128)S(1)} %get-tuple-element.423), kind=kLoop, calls=%fused_computation.38 | loop fusion | flops 4194304 | bytes 25198592 | tf_op jit(solution)/shard_map/while/body/eval_jaxpr/cond/branch_1_fun/add | solution.py:73
  166.1 4.0 %select_convert_fusion = bf16[8,512,256]{2,1,0:T(8,128)(2,1)S(1)} fusion(f32[8,1024,256]{2,1,0:T(8,128)} %get-tuple-element.413, pred[]{:T(512)S(6)} %eq.17), kind=kLoop, calls=%fused_computation.51 | loop fusion | flops 1048576 | bytes 6291457 | tf_op jit(solution)/shard_map/convert_element_type | solution.py:36
  170.4 0.7 convolution_convert_fusion.4
  171.2 3.1 %collective-permute-start.14 = (bf16[15,512]{1,0:T(8,128)(2,1)S(1)}, bf16[15,512]{1,0:T(8,128)(2,1)S(1)}, u32[]{:S(2)}, u32[]{:S(2)}) collective-permute-start(bf16[15,512]{1,0:T(8,128)(2,1)S(1)} %slice.241), channel_id=1, source_target_pairs={{0,2},{2,4},{4,6},{6,8},{8,10},{10,12},{12,14},{14,16},{16,18},{18... | collective-permute-start | bytes 46088 | tf_op jit(solution)/shard_map/ppermute | solution.py:15
  174.3 1.4 collective-permute-start.12
  175.8 1.7 collective-permute-done.14
  177.6 38.3 %collective-permute-done.12 = bf16[8,512]{1,0:T(8,128)(2,1)S(1)} collective-permute-done((bf16[8,512]{1,0:T(8,128)(2,1)S(1)}, bf16[8,512]{1,0:T(8,128)(2,1)S(1)}, u32[]{:S(2)}, u32[]{:S(2)}) %collective-permute-start.12) | collective-permute-done | bytes 8224 | tf_op jit(solution)/shard_map/ppermute | solution.py:25
  216.2 4.7 %multiply_add_fusion.4 = f32[8,512,256]{2,1,0:T(8,128)S(1)} fusion(bf16[8,512,256]{2,1,0:T(8,128)(2,1)S(1)} %collective-permute-done.9, f32[8,1024,256]{2,1,0:T(8,128)} %get-tuple-element.413, f32[8,512]{1,0:T(8,128)S(1)} %get-tuple-element.429, f32[8,512]{1,0:T(8,128)S(1)} %get-tuple-element.428, pred[]{:T(512)S(6)} %eq.17), kind=kLoop, calls=%fused_computation.50 | loop fusion | flops 5242880 | bytes 14712833 | tf_op jit(solution)/shard_map/add | solution.py:110
  221.0 0.9 collective-permute-start.11
  221.9 0.6 collective-permute-start.13
  222.6 0.8 collective-permute-start.10
  223.4 1.3 convolution_convert_fusion.3
  224.7 18.4 %collective-permute-done.13 = bf16[8,256]{1,0:T(8,128)(2,1)S(1)} collective-permute-done((bf16[8,256]{1,0:T(8,128)(2,1)S(1)}, bf16[8,256]{1,0:T(8,128)(2,1)S(1)}, u32[]{:S(2)}, u32[]{:S(2)}) %collective-permute-start.13) | collective-permute-done | bytes 4128 | tf_op jit(solution)/shard_map/ppermute | solution.py:25
  243.2 1.0 divide_convert_fusion
  244.4 0.3 multiply_reduce_fusion
  244.9 0.2 fusion.26
  245.4 3.5 %fusion.60 = f32[256,2048]{1,0:T(8,128)S(1)} fusion(bf16[256,1024]{0,1:T(8,128)(2,1)S(1)} %bitcast.113, bf16[1024,2048]{1,0:T(8,128)(2,1)} %param.26), kind=kOutput, calls=%fused_computation.159 | convolution fusion | flops 1073741824 | bytes 6815744 | tf_op jit(solution)/shard_map/dot_general | solution.py:230
  248.8 1.7 fusion.22
  250.6 11.9 %reduce-scatter.2.cloned.1.call-done = bf16[128,2048]{1,0:T(8,128)(2,1)} async-done(((bf16[256,2048]{1,0:T(8,128)(2,1)}), bf16[128,2048]{1,0:T(8,128)(2,1)}) %reduce-scatter.2.cloned.1.call-update) | async-done | bytes 524304 | tf_op jit(solution)/shard_map/reduce_scatter | solution.py:231
  (88 shorter events, 2.6 us)
Async XLA Ops:
  6.5 242.3 %copy-start = (bf16[512,2048]{1,0:T(8,128)(2,1)S(1)}, bf16[512,2048]{1,0:T(8,128)(2,1)}, u32[]{:S(2)}) copy-start(bf16[512,2048]{1,0:T(8,128)(2,1)} %param.27) | copy-start | bytes 6291460
  6.5 13.1 %all-gather.2.cloned.1.call-start = ((), (), s32[]{:S(2)}) async-start(), calls=%async_computation.1 | async-start | bytes 1572864 | tf_op jit(solution)/shard_map/all_gather | solution.py:136
  7.3 255.2 %reduce-scatter.2.cloned.1.call-start = ((), (), s32[]{:S(2)}) async-start(), calls=%async_computation.2 | async-start | bytes 1572864 | tf_op jit(solution)/shard_map/reduce_scatter | solution.py:231
  23.5 1.3 copy-start.2
  23.5 13.4 %collective-permute-start = (bf16[256,8,128]{2,0,1:T(8,128)(2,1)S(1)}, bf16[256,8,128]{2,0,1:T(8,128)(2,1)}, u32[]{:S(2)}, u32[]{:S(2)}) collective-permute-start(bf16[256,8,128]{2,0,1:T(8,128)(2,1)S(1)} %bitcast.109), channel_id=1, source_target_pairs={{0,2},{2,0},{4,6},{6,4},{8,10},{10,8},{12,14},{14,12},{16,18},{18,... | collective-permute-start | bytes 1572872 | tf_op jit(solution)/shard_map/ppermute | solution.py:25
  38.8 6.3 %copy-start.9 = (bf16[2048,1024]{1,0:T(8,128)(2,1)S(1)}, bf16[2048,1024]{1,0:T(8,128)(2,1)}, u32[]{:S(2)}) copy-start(bf16[2048,1024]{1,0:T(8,128)(2,1)} %param.21) | copy-start | bytes 12582916
  38.8 6.3 %copy-start.11 = (bf16[256,2048]{1,0:T(8,128)(2,1)S(1)}, bf16[256,2048]{1,0:T(8,128)(2,1)}, u32[]{:S(2)}) copy-start(bf16[256,2048]{1,0:T(8,128)(2,1)} %all-gather.2.cloned.1.call-done) | copy-start | bytes 3145732
  38.9 23.8 %collective-permute-start.1 = (bf16[512,8,128]{2,0,1:T(8,128)(2,1)S(1)}, bf16[512,8,128]{2,0,1:T(8,128)(2,1)S(1)}, u32[]{:S(2)}, u32[]{:S(2)}) collective-permute-start(bf16[512,8,128]{2,0,1:T(8,128)(2,1)S(1)} %maximum_select_fusion.1), channel_id=1, source_target_pairs={{0,4},{4,0},{2,6},{6,2},{8,12},{12,8},{10,14},{14,10},{16,20},{20,... | collective-permute-start | bytes 3145736 | tf_op jit(solution)/shard_map/ppermute | solution.py:25
  44.2 2.3 copy-start.3
  45.2 18.8 %copy-start.14 = (f32[8]{0:T(128)S(1)}, f32[8]{0:T(128)}, u32[]{:S(2)}) copy-start(f32[8]{0:T(128)} %param.24) | copy-start | bytes 100
  45.2 12.6 %collective-permute-start.2 = (bf16[256,8,128]{2,0,1:T(8,128)(2,1)}, bf16[256,8,128]{2,0,1:T(8,128)(2,1)S(1)}, u32[]{:S(2)}, u32[]{:S(2)}) collective-permute-start(bf16[256,8,128]{2,0,1:T(8,128)(2,1)} %copy_bitcast_fusion.1), channel_id=1, source_target_pairs={{0,8},{2,10},{4,12},{6,14},{8,16},{10,18},{12,20},{14,22},{16,24},... | collective-permute-start | bytes 1572872 | tf_op jit(solution)/shard_map/ppermute | solution.py:30
  46.5 16.2 %copy-start.4 = (bf16[256,1024]{1,0:T(8,128)(2,1)}, bf16[256,1024]{1,0:T(8,128)(2,1)S(1)}, u32[]{:S(2)}) copy-start(bf16[256,1024]{1,0:T(8,128)(2,1)S(1)} %convolution_convert_fusion) | copy-start | bytes 1572868
  47.3 42.2 %collective-permute-start.3 = (bf16[256,4,256]{2,0,1:T(8,128)(2,1)}, bf16[256,4,256]{2,0,1:T(8,128)(2,1)}, u32[]{:S(2)}, u32[]{:S(2)}) collective-permute-start(bf16[256,4,256]{2,0,1:T(8,128)(2,1)} %bitcast.100), channel_id=1, source_target_pairs={{0,8},{2,10},{4,12},{6,14},{8,16},{10,18},{12,20},{14,22},{16,24},... | collective-permute-start | bytes 1572872 | tf_op jit(solution)/shard_map/ppermute | solution.py:30
  48.8 76.5 %collective-permute-start.4 = (bf16[256,8,128]{2,0,1:T(8,128)(2,1)}, bf16[256,8,128]{2,0,1:T(8,128)(2,1)}, u32[]{:S(2)}, u32[]{:S(2)}) collective-permute-start(bf16[256,8,128]{2,0,1:T(8,128)(2,1)} %copy_bitcast_fusion.1), channel_id=1, source_target_pairs={{0,16},{2,18},{4,20},{6,22},{8,24},{10,26},{12,28},{14,30},{16,0},... | collective-permute-start | bytes 1572872 | tf_op jit(solution)/shard_map/ppermute | solution.py:30
  50.0 86.5 %collective-permute-start.5 = (bf16[256,4,256]{2,0,1:T(8,128)(2,1)}, bf16[256,4,256]{2,0,1:T(8,128)(2,1)}, u32[]{:S(2)}, u32[]{:S(2)}) collective-permute-start(bf16[256,4,256]{2,0,1:T(8,128)(2,1)} %bitcast.100), channel_id=1, source_target_pairs={{0,16},{2,18},{4,20},{6,22},{8,24},{10,26},{12,28},{14,30},{16,0},... | collective-permute-start | bytes 1572872 | tf_op jit(solution)/shard_map/ppermute | solution.py:30
  57.8 4.9 %copy-start.6 = (bf16[256,8,128]{2,0,1:T(8,128)(2,1)}, bf16[256,8,128]{2,0,1:T(8,128)(2,1)S(1)}, u32[]{:S(2)}) copy-start(bf16[256,8,128]{2,0,1:T(8,128)(2,1)S(1)} %collective-permute-done.2) | copy-start | bytes 1572868
  57.8 93.4 %collective-permute-start.6 = (bf16[256,8,128]{2,0,1:T(8,128)(2,1)}, bf16[256,8,128]{2,0,1:T(8,128)(2,1)}, u32[]{:S(2)}, u32[]{:S(2)}) collective-permute-start(bf16[256,8,128]{2,0,1:T(8,128)(2,1)} %copy_bitcast_fusion.1), channel_id=1, source_target_pairs={{0,24},{2,26},{4,28},{6,30},{8,0},{10,2},{12,4},{14,6},{16,8},{18,... | collective-permute-start | bytes 1572872 | tf_op jit(solution)/shard_map/ppermute | solution.py:30
  62.7 1.0 copy-start.5
  63.7 87.5 %collective-permute-start.7 = (bf16[256,4,256]{2,0,1:T(8,128)(2,1)}, bf16[256,4,256]{2,0,1:T(8,128)(2,1)}, u32[]{:S(2)}, u32[]{:S(2)}) collective-permute-start(bf16[256,4,256]{2,0,1:T(8,128)(2,1)} %bitcast.100), channel_id=1, source_target_pairs={{0,24},{2,26},{4,28},{6,30},{8,0},{10,2},{12,4},{14,6},{16,8},{18,... | collective-permute-start | bytes 1572872 | tf_op jit(solution)/shard_map/ppermute | solution.py:30
  75.7 13.8 %copy-start.7 = (bf16[256,8,128]{2,0,1:T(8,128)(2,1)S(1)}, bf16[256,8,128]{2,0,1:T(8,128)(2,1)}, u32[]{:S(2)}) copy-start(bf16[256,8,128]{2,0,1:T(8,128)(2,1)} %copy-done.6) | copy-start | bytes 1572868
  79.2 2.1 copy-start.1
  166.1 4.2 %copy-start.10 = (bf16[2048,512]{1,0:T(8,128)(2,1)S(1)}, bf16[2048,512]{1,0:T(8,128)(2,1)}, u32[]{:S(2)}) copy-start(bf16[2048,512]{1,0:T(8,128)(2,1)} %param.22) | copy-start | bytes 6291460
  166.1 4.3 %copy-start.12 = (bf16[256,2048]{1,0:T(8,128)(2,1)S(1)}, bf16[256,2048]{1,0:T(8,128)(2,1)}, u32[]{:S(2)}) copy-start(bf16[256,2048]{1,0:T(8,128)(2,1)} %all-gather.2.cloned.1.call-done) | copy-start | bytes 3145732
  170.1 46.0 %collective-permute-start.9 = (bf16[8,512,256]{2,1,0:T(8,128)(2,1)S(1)}, bf16[8,512,256]{2,1,0:T(8,128)(2,1)S(1)}, u32[]{:S(2)}, u32[]{:S(2)}) collective-permute-start(bf16[8,512,256]{2,1,0:T(8,128)(2,1)S(1)} %select_convert_fusion), channel_id=1, source_target_pairs={{0,4},{4,0},{2,6},{6,2},{8,12},{12,8},{10,14},{14,10},{16,20},{20,... | collective-permute-start | bytes 6291464 | tf_op jit(solution)/shard_map/ppermute | solution.py:25
  171.2 6.4 %collective-permute-start.14 = (bf16[15,512]{1,0:T(8,128)(2,1)S(1)}, bf16[15,512]{1,0:T(8,128)(2,1)S(1)}, u32[]{:S(2)}, u32[]{:S(2)}) collective-permute-start(bf16[15,512]{1,0:T(8,128)(2,1)S(1)} %slice.241), channel_id=1, source_target_pairs={{0,2},{2,4},{4,6},{6,8},{8,10},{10,12},{12,14},{14,16},{16,18},{18... | collective-permute-start | bytes 46088 | tf_op jit(solution)/shard_map/ppermute | solution.py:15
  174.3 41.7 %collective-permute-start.12 = (bf16[8,512]{1,0:T(8,128)(2,1)S(1)}, bf16[8,512]{1,0:T(8,128)(2,1)S(1)}, u32[]{:S(2)}, u32[]{:S(2)}) collective-permute-start(bf16[8,512]{1,0:T(8,128)(2,1)S(1)} %select_convert_fusion.2), channel_id=1, source_target_pairs={{0,4},{4,0},{2,6},{6,2},{8,12},{12,8},{10,14},{14,10},{16,20},{20,... | collective-permute-start | bytes 24584 | tf_op jit(solution)/shard_map/ppermute | solution.py:25
  175.7 40.4 %collective-permute-start.8 = (bf16[8,512]{1,0:T(8,128)(2,1)S(1)}, bf16[8,512]{1,0:T(8,128)(2,1)S(1)}, u32[]{:S(2)}, u32[]{:S(2)}) collective-permute-start(bf16[8,512]{1,0:T(8,128)(2,1)S(1)} %select_convert_fusion.3), channel_id=1, source_target_pairs={{0,4},{4,0},{2,6},{6,2},{8,12},{12,8},{10,14},{14,10},{16,20},{20,... | collective-permute-start | bytes 24584 | tf_op jit(solution)/shard_map/ppermute | solution.py:25
  216.2 7.3 %copy-start.13 = (bf16[4,128,128]{2,1,0:T(8,128)(2,1)S(1)}, bf16[4,128,128]{2,1,0:T(8,128)(2,1)}, u32[]{:S(2)}) copy-start(bf16[4,128,128]{2,1,0:T(8,128)(2,1)} %param.23) | copy-start | bytes 393220
  221.0 22.2 %collective-permute-start.11 = (bf16[8,256,256]{2,1,0:T(8,128)(2,1)S(1)}, bf16[8,256,256]{2,1,0:T(8,128)(2,1)S(1)}, u32[]{:S(2)}, u32[]{:S(2)}) collective-permute-start(bf16[8,256,256]{2,1,0:T(8,128)(2,1)S(1)} %select_convert_fusion.1), channel_id=1, source_target_pairs={{0,2},{2,0},{4,6},{6,4},{8,10},{10,8},{12,14},{14,12},{16,18},{18,... | collective-permute-start | bytes 3145736 | tf_op jit(solution)/shard_map/ppermute | solution.py:25
  221.9 21.2 %collective-permute-start.13 = (bf16[8,256]{1,0:T(8,128)(2,1)S(1)}, bf16[8,256]{1,0:T(8,128)(2,1)S(1)}, u32[]{:S(2)}, u32[]{:S(2)}) collective-permute-start(bf16[8,256]{1,0:T(8,128)(2,1)S(1)} %select_convert_fusion.4), channel_id=1, source_target_pairs={{0,2},{2,0},{4,6},{6,4},{8,10},{10,8},{12,14},{14,12},{16,18},{18,... | collective-permute-start | bytes 12296 | tf_op jit(solution)/shard_map/ppermute | solution.py:25
  222.6 20.6 %collective-permute-start.10 = (bf16[8,256]{1,0:T(8,128)(2,1)S(1)}, bf16[8,256]{1,0:T(8,128)(2,1)S(1)}, u32[]{:S(2)}, u32[]{:S(2)}) collective-permute-start(bf16[8,256]{1,0:T(8,128)(2,1)S(1)} %select_convert_fusion.5), channel_id=1, source_target_pairs={{0,2},{2,0},{4,6},{6,4},{8,10},{10,8},{12,14},{14,12},{16,18},{18,... | collective-permute-start | bytes 12296 | tf_op jit(solution)/shard_map/ppermute | solution.py:25
  244.2 0.7 copy-start.8
Sparse Core Ops, SparseCore 0:
  8.9 10.7 all-gather.1
  250.7 11.7 reduce-scatter.1
where the time goes:
time: 271 us; the launch traced here: 269 us
  waiting for transfers between devices  139 us (51%)
  other arithmetic  51.1 us (19%)
  matrix products  39 us (14%)
  starting transfers between devices  13.9 us (5%)
  between operations  13.7 us (5%)
  local copies, waits for them, and re-layouts  11.8 us (4%)
    ppermute x8, waiting for transfers between devices, from_partner(): return lax.ppermute(block, axis, route)  73.8 us
    ppermute x6, waiting for transfers between devices, shifted(): lax.ppermute(array, axis, [(i, (i + by) % size) for i in range(size)])  38.8 us
    add x4, other arithmetic, block_work(): weighted * shrink[:, :, None] + update.reshape(unit_count, query_count, -1)  25.8 us
    dot_general x4, matrix products, block_work(): jnp.einsum('qud,kud->uqk', queries, key_rows, preferred_element_type=jnp....  12.5 us
    all_gather x1, waiting for transfers between devices, per_device(): project_incoming = lax.all_gather(normed, 'tp', axis=0, tiled=True)  12.3 us
    reduce_scatter x1, waiting for transfers between devices, per_device(): lax.psum_scatter((partial_value + jnp.dot(pool_out, pool_out_weight, pref...  11.9 us
    dot_general x4, matrix products, block_work(): jnp.einsum('hmqk,khe->hmqe', map_weights, value_rows, preferred_element_t...  10.2 us
    dot_general x4, matrix products, per_device(): jnp.dot(project_incoming, weight_part, preferred_element_type=jnp.float32)  9.77 us
  transfers between devices with their start and end apart: 17, of which 12 were waited for; matrix products, arithmetic and copies ran while one was open for 24% of the time, Pallas kernels for 0%

commit v1 on v0

--- a/solution.py
+++ b/solution.py
@@ -1,8 +1,11 @@
+import functools
 import math
 
 import jax
 import jax.numpy as jnp
 from jax import lax
+from jax.experimental import pallas as pl
+from jax.experimental.pallas import tpu as pltpu
 from jax.sharding import PartitionSpec as P
 
 reach_back = 15
@@ -238,9 +241,548 @@
     )
 
 
+MESH = pl.DeviceIdType.MESH
+
+
+def flipped(index, mask, size):
+    total = 0
+    bit = 1
+    while bit < size:
+        total = total + lax.rem(lax.div(index, bit) + lax.div(mask, bit), 2) * bit
+        bit *= 2
+    return total
+
+
+def layer_kernel(
+    sp_count,
+    members,
+    x_ref,
+    pool_weight,
+    balance,
+    gain,
+    query_hbm,
+    key_hbm,
+    value_hbm,
+    pool_in_hbm,
+    contrast_hbm,
+    pool_out_hbm,
+    out_ref,
+    query_w,
+    key_w,
+    value_w,
+    pool_in_w,
+    contrast_w,
+    pool_out_w,
+    rows_in,
+    kv,
+    kv_stage,
+    queries,
+    query_stage,
+    peaks,
+    totals,
+    weighted,
+    contrasts,
+    contrast_stage,
+    rim,
+    rim_stage,
+    pool_part,
+    out_stage,
+    out_recv,
+    weight_sem,
+    local_sem,
+    pair_send,
+    pair_recv,
+    relay_send,
+    relay_recv,
+    kv_send,
+    kv_recv,
+    query_send,
+    query_recv,
+    contrast_send,
+    contrast_recv,
+    rim_send,
+    rim_recv,
+    out_send,
+    out_recv_sem,
+):
+    f32 = jnp.float32
+    bf16 = jnp.bfloat16
+    bands = sp_count // members
+    sp = lax.axis_index("sp")
+    tp = lax.axis_index("tp")
+    other = 1 - tp
+    band = lax.div(sp, members)
+    member = lax.rem(sp, members)
+    half, model = x_ref.shape
+    rows = 2 * half
+    width = gain.shape[1]
+    head_dim = width // 2
+
+    loads = [
+        pltpu.make_async_copy(src, dst, weight_sem.at[i])
+        for i, (src, dst) in enumerate(
+            (
+                (key_hbm, key_w),
+                (value_hbm, value_w),
+                (query_hbm, query_w),
+                (pool_in_hbm, pool_in_w),
+                (pool_out_hbm, pool_out_w),
+                (contrast_hbm, contrast_w),
+            )
+        )
+    ]
+    for load in loads:
+        load.start()
+    keep = pltpu.make_async_copy(x_ref, rows_in.at[0, tp], local_sem)
+    keep.start()
+
+    barrier = pltpu.get_barrier_semaphore()
+    greeted = [
+        (sp, other),
+        (lax.rem(sp + members, sp_count), tp),
+        (lax.rem(sp + sp_count - members, sp_count), tp),
+        (lax.rem(sp + 1, sp_count), tp),
+        (lax.rem(sp + sp_count - 1, sp_count), tp),
+    ]
+    greeted += [(band * members + flipped(member, j, members), tp) for j in range(1, members)]
+    for target in greeted:
+        pl.semaphore_signal(barrier, inc=1, device_id=target, device_id_type=MESH)
+    pl.semaphore_wait(barrier, len(greeted))
+
+    def pair_copy(step):
+        return pltpu.make_async_remote_copy(
+            src_ref=x_ref if step == 0 else rows_in.at[step, tp],
+            dst_ref=rows_in.at[step, tp],
+            send_sem=pair_send.at[step],
+            recv_sem=pair_recv.at[step],
+            device_id=(sp, other),
+            device_id_type=MESH,
+        )
+
+    def relay_copy(step):
+        return pltpu.make_async_remote_copy(
+            src_ref=x_ref if step == 1 else rows_in.at[step - 1, tp],
+            dst_ref=rows_in.at[step, tp],
+            send_sem=relay_send.at[step],
+            recv_sem=relay_recv.at[step],
+            device_id=(lax.rem(sp + members, sp_count), tp),
+            device_id_type=MESH,
+        )
+
+    def kv_copy(step, j):
+        return pltpu.make_async_remote_copy(
+            src_ref=kv_stage.at[step, j],
+            dst_ref=kv.at[step, member],
+            send_sem=kv_send.at[step, j],
+            recv_sem=kv_recv.at[step, j],
+            device_id=(band * members + flipped(member, j, members), tp),
+            device_id_type=MESH,
+        )
+
+    def query_copy(j):
+        return pltpu.make_async_remote_copy(
+            src_ref=query_stage.at[j],
+            dst_ref=queries.at[member],
+            send_sem=query_send.at[j],
+            recv_sem=query_recv.at[j],
+            device_id=(band * members + flipped(member, j, members), tp),
+            device_id_type=MESH,
+        )
+
+    def contrast_copy(j):
+        return pltpu.make_async_remote_copy(
+            src_ref=contrast_stage.at[j],
+            dst_ref=contrasts.at[member],
+            send_sem=contrast_send.at[j],
+            recv_sem=contrast_recv.at[j],
+            device_id=(band * members + flipped(member, j, members), tp),
+            device_id_type=MESH,
+        )
+
+    rim_copy = pltpu.make_async_remote_copy(
+        src_ref=rim_stage,
+        dst_ref=rim,
+        send_sem=rim_send,
+        recv_sem=rim_recv,
+        device_id=(lax.rem(sp + 1, sp_count), tp),
+        device_id_type=MESH,
+    )
+    out_copy = pltpu.make_async_remote_copy(
+        src_ref=out_stage,
+        dst_ref=out_recv,
+        send_sem=out_send,
+        recv_sem=out_recv_sem,
+        device_id=(sp, other),
+        device_id_type=MESH,
+    )
+
+    pair_copy(0).start()
+
+    @pl.when(band + 1 < bands)
+    def _():
+        relay_copy(1).start()
+
+    def project(step):
+        def one(t, carry):
+            j = members - 1 - t
+            head = flipped(member, j, members)
+            columns = pl.ds(pl.multiple_of(head * width, width), width)
+            x = rows_in[step].reshape(rows, model)
+            keys = jnp.dot(x, key_w[:, columns], preferred_element_type=f32).astype(bf16)
+            values = jnp.dot(x, value_w[:, columns], preferred_element_type=f32).astype(bf16)
+
+            @pl.when(j > 0)
+            def _():
+                kv_stage[step, j, :, :width] = keys
+                kv_stage[step, j, :, width:] = values
+                kv_copy(step, j).start()
+
+            @pl.when(j == 0)
+            def _():
+                kv[step, member, :, :width] = keys
+                kv[step, member, :, width:] = values
+
+            if step == 0:
+                mine = jnp.dot(x, query_w[:, columns], preferred_element_type=f32).astype(bf16)
+
+                @pl.when(j > 0)
+                def _():
+                    query_stage[j] = mine
+                    query_copy(j).start()
+
+                @pl.when(j == 0)
+                def _():
+                    queries[member] = mine
+
+            return carry
+
+        lax.fori_loop(0, members, one, 0)
+
+    def take_band(step):
+        @pl.when(band >= step)
+        def _():
+            relay_copy(step).wait_recv()
+            if step + 1 < bands:
+
+                @pl.when(band + 1 < bands)
+                def _():
+                    relay_copy(step + 1).start()
+
+            pair_copy(step).start()
+            pair_copy(step).wait_recv()
+            project(step)
+
+    log_scale = head_dim ** (-0.5) * math.log2(math.e)
+
+    def attend_block(step, i, seen):
+        for u in range(2):
+            cols = slice(u * head_dim, (u + 1) * head_dim)
+            keys = kv[step, :seen, :, cols].reshape(seen * rows, head_dim)
+            values = kv[step, :seen, :, width:].reshape(seen * rows, width)
+            scores = lax.dot_general(
+                queries[i, :, cols], keys, (((1,), (1,)), ((), ())), preferred_element_type=f32
+            )
+            if step == 0:
+                query_order = lax.broadcasted_iota(jnp.int32, scores.shape, 0) + (seen - 1) * rows
+                key_order = lax.broadcasted_iota(jnp.int32, scores.shape, 1)
+                scores = jnp.where(key_order <= query_order, scores, -jnp.inf)
+            peak = jnp.max(scores, axis=1, keepdims=True)
+            if step > 0:
+                old = peaks[u, i][:, :1]
+                peak = jnp.maximum(peak, old)
+                shrink = jnp.exp2((old - peak) * log_scale)
+            raised = jnp.exp2((scores - peak) * log_scale)
+            total = jnp.sum(raised, axis=1, keepdims=True)
+            update = jnp.dot(raised.astype(bf16), values, preferred_element_type=f32)
+            if step > 0:
+                total = total + totals[u, i][:, :1] * shrink
+                update = update + weighted[u, i] * shrink
+            peaks[u, i] = jnp.broadcast_to(peak, peaks.shape[2:])
+            totals[u, i] = jnp.broadcast_to(total, totals.shape[2:])
+            weighted[u, i] = update
+
+    def attend_own():
+        for j in range(1, members):
+            query_copy(j).wait_recv()
+            kv_copy(0, j).wait_recv()
+        for i in range(members):
+            attend_block(0, i, i + 1)
+
+    def attend_band(step):
+        @pl.when(band >= step)
+        def _():
+            for j in range(1, members):
+                kv_copy(step, j).wait_recv()
+
+            def one(i, carry):
+                attend_block(step, i, members)
+                return carry
+
+            lax.fori_loop(0, members, one, 0)
+
+    keep.wait()
+    loads[0].wait()
+    loads[1].wait()
+    loads[2].wait()
+    pair_copy(0).wait_recv()
+    project(0)
+
+    loads[3].wait()
+    pool_input = jnp.dot(
+        rows_in[0].reshape(rows, model), pool_in_w[...], preferred_element_type=f32
+    ).astype(bf16)
+    rim_stage[...] = pool_input[rows - rim.shape[0] :]
+
+    @pl.when(sp + 1 < sp_count)
+    def _():
+        rim_copy.start()
+
+    take_band(1)
+
+    @pl.when(sp > 0)
+    def _():
+        rim_copy.wait_recv()
+
+    @pl.when(sp == 0)
+    def _():
+        rim[...] = jnp.zeros_like(rim)
+
+    loads[4].wait()
+    extended = jnp.concatenate([rim[...], pool_input], axis=0).astype(f32)
+    group_width = pool_weight.shape[1]
+    skirt = rim.shape[0]
+    position = sp * rows + lax.broadcasted_iota(jnp.int32, (rows, group_width), 0)
+    mixed = []
+    for group in range(pool_weight.shape[0]):
+        block = extended[:, group * group_width : (group + 1) * group_width]
+        window = block
+        reach = 1
+        span = 2 ** (1 + group % 4)
+        while reach < span:
+            window = window + pltpu.roll(window, reach, 0)
+            reach *= 2
+        counts = jnp.minimum(position + 1, span).astype(f32)
+        spread = (window[skirt:] / counts - block[skirt:]).astype(bf16)
+        mixed.append(
+            jnp.dot(spread, pool_weight[group], preferred_element_type=f32).astype(bf16)
+        )
+    pool_out = jnp.concatenate(mixed, axis=1)
+    chunk = math.gcd(model, 512)
+    for start in range(0, model, chunk):
+        pool_part[:, start : start + chunk] = jnp.dot(
+            pool_out, pool_out_w[:, start : start + chunk], preferred_element_type=f32
+        )
+
+    for step in range(2, bands):
+        take_band(step)
+        if step == 2:
+            attend_own()
+        else:
+            attend_band(step - 2)
+    if bands == 2:
+        attend_own()
+    for step in range(max(bands - 2, 1), bands):
+        attend_band(step)
+
+    weight = balance[tp * members + member]
+
+    def finish(t, carry):
+        j = members - 1 - t
+        i = flipped(member, j, members)
+        first = (weighted[0, i] / totals[0, i][:, :1]).astype(bf16).astype(f32)
+        second = (weighted[1, i] / totals[1, i][:, :1]).astype(bf16).astype(f32)
+        contrast = first - weight * second
+        mean_square = jnp.mean(contrast * contrast, axis=1, keepdims=True)
+        result = (contrast * lax.rsqrt(mean_square + norm_epsilon) * gain[...]).astype(bf16)
+
+        @pl.when(j > 0)
+        def _():
+            contrast_stage[j] = result
+            contrast_copy(j).start()
+
+        @pl.when(j == 0)
+        def _():
+            contrasts[member] = result
+
+        return carry
+
+    lax.fori_loop(0, members, finish, 0)
+    loads[5].wait()
+    for j in range(1, members):
+        contrast_copy(j).wait_recv()
+
+    def projected(side, store):
+        taken = pl.ds(pl.multiple_of(side * half, half), half)
+        left = jnp.concatenate([contrasts[h, taken, :] for h in range(members)], axis=1)
+        for start in range(0, model, chunk):
+            cut = slice(start, start + chunk)
+            part = jnp.dot(left, contrast_w[:, cut], preferred_element_type=f32)
+            store(cut, (part + pool_part[taken, cut]).astype(bf16))
+
+    def to_partner(cut, part):
+        out_stage[:, cut] = part
+
+    def to_self(cut, part):
+        out_ref[:, cut] = part
+
+    projected(other, to_partner)
+    out_copy.start()
+    projected(tp, to_self)
+    out_copy.wait()
+    out_ref[...] = (out_ref[...].astype(f32) + out_recv[...].astype(f32)).astype(bf16)
+
+    pair_copy(0).wait_send()
+    for j in range(1, members):
+        query_copy(j).wait_send()
+        kv_copy(0, j).wait_send()
+        contrast_copy(j).wait_send()
+
+    @pl.when(sp + 1 < sp_count)
+    def _():
+        rim_copy.wait_send()
+
+    for step in range(1, bands):
+
+        @pl.when(jnp.logical_and(band + 1 < bands, band >= step - 1))
+        def _(step=step):
+            relay_copy(step).wait_send()
+
+        @pl.when(band >= step)
+        def _(step=step):
+            pair_copy(step).wait_send()
+            for j in range(1, members):
+                kv_copy(step, j).wait_send()
+
+
+def kernel_scratch(sp_count, members, half, model, width, pool_cols):
+    bf16 = jnp.bfloat16
+    bands = sp_count // members
+    rows = 2 * half
+    columns = members * width
+    dma = pltpu.SemaphoreType.DMA
+    return [
+        pltpu.VMEM((model, columns), bf16),
+        pltpu.VMEM((model, columns), bf16),
+        pltpu.VMEM((model, columns), bf16),
+        pltpu.VMEM((model, pool_cols), bf16),
+        pltpu.VMEM((columns, model), bf16),
+        pltpu.VMEM((pool_cols, model), bf16),
+        pltpu.VMEM((bands, 2, half, model), bf16),
+        pltpu.VMEM((bands, members, rows, 2 * width), bf16),
+        pltpu.VMEM((bands, members, rows, 2 * width), bf16),
+        pltpu.VMEM((members, rows, width), bf16),
+        pltpu.VMEM((members, rows, width), bf16),
+        pltpu.VMEM((2, members, rows, 128), jnp.float32),
+        pltpu.VMEM((2, members, rows, 128), jnp.float32),
+        pltpu.VMEM((2, members, rows, width), jnp.float32),
+        pltpu.VMEM((members, rows, width), bf16),
+        pltpu.VMEM((members, rows, width), bf16),
+        pltpu.VMEM((reach_back + 1, pool_cols), bf16),
+        pltpu.VMEM((reach_back + 1, pool_cols), bf16),
+        pltpu.VMEM((rows, model), jnp.float32),
+        pltpu.VMEM((half, model), bf16),
+        pltpu.VMEM((half, model), bf16),
+        dma((6,)),
+        dma,
+        dma((bands,)),
+        dma((bands,)),
+        dma((bands,)),
+        dma((bands,)),
+        dma((bands, members)),
+        dma((bands, members)),
+        dma((members,)),
+        dma((members,)),
+        dma((members,)),
+        dma((members,)),
+        dma,
+        dma,
+        dma,
+        dma,
+    ]
+
+
+vmem_most = 67043328
+
+
+def scratch_bytes(scratch):
+    return sum(
+        math.prod(item.shape) * jnp.dtype(item.dtype).itemsize
+        for item in scratch
+        if getattr(item, "memory_space", None) == pltpu.VMEM
+    )
+
+
+def whole_layer(
+    normed,
+    query_weight,
+    key_weight,
+    value_weight,
+    pool_in_weight,
+    pool_weight,
+    map_balance,
+    head_gain,
+    contrast_out_weight,
+    pool_out_weight,
+):
+    sp_count = lax.axis_size("sp")
+    width = head_gain.shape[0]
+    members = query_weight.shape[1] // width
+    half, model = normed.shape
+    pool_cols = pool_in_weight.shape[1]
+    groups_here = pool_weight.shape[0]
+    scratch = kernel_scratch(
+        sp_count, max(members, 1), half, model, width, pool_cols
+    )
+    fits = (
+        lax.axis_size("tp") == 2
+        and members > 1
+        and members & (members - 1) == 0
+        and sp_count % members == 0
+        and sp_count // members > 1
+        and groups_here % 4 == 0
+        and scratch_bytes(scratch) < vmem_most * 3 // 4
+    )
+    if not fits:
+        return per_device(
+            normed,
+            query_weight,
+            key_weight,
+            value_weight,
+            pool_in_weight,
+            pool_weight,
+            map_balance,
+            head_gain,
+            contrast_out_weight,
+            pool_out_weight,
+        )
+    vmem = pl.BlockSpec(memory_space=pltpu.VMEM)
+    hbm = pl.BlockSpec(memory_space=pl.ANY)
+    return pl.pallas_call(
+        functools.partial(layer_kernel, sp_count, members),
+        out_shape=jax.ShapeDtypeStruct((half, model), jnp.bfloat16),
+        in_specs=[vmem, vmem, pl.BlockSpec(memory_space=pltpu.SMEM), vmem] + [hbm] * 6,
+        out_specs=vmem,
+        scratch_shapes=scratch,
+        compiler_params=pltpu.CompilerParams(
+            collective_id=0, has_side_effects=True, vmem_limit_bytes=vmem_most
+        ),
+    )(
+        normed,
+        pool_weight,
+        map_balance,
+        head_gain.reshape(1, width),
+        query_weight,
+        key_weight,
+        value_weight,
+        pool_in_weight,
+        contrast_out_weight,
+        pool_out_weight,
+    )
+
+
 def solution(mesh):
     return jax.shard_map(
-        per_device,
+        whole_layer,
         mesh=mesh,
         in_specs=(
             P(("sp", "tp"), None),

time: 271 us -> 79.9 us (0.29)
  waiting for transfers between devices: 139 us -> 0 us
  Pallas kernels: 0 us -> 77.5 us
  other arithmetic: 51.1 us -> 0 us
  matrix products: 39 us -> 0 us
  starting transfers between devices: 13.9 us -> 0 us
  between operations: 13.7 us -> 0.01 us
  local copies, waits for them, and re-layouts: 11.8 us -> 1.88 us
    ppermute x15 -> x0, waiting for transfers between devices: 114 us -> none  [the longest x8 73.8 us: from_partner(): return lax.ppermute(block, axis, route)]
    pallas_call x0 -> x1, Pallas kernels: none -> 77.5 us  [whole_layer(): pl.pallas_call(functools.partial(layer_kernel, sp_count, members), out_sh...]
    dot_general x15 -> x0, matrix products: 39 us -> none  [the longest x4 12.5 us: block_work(): jnp.einsum('qud,kud->uqk', queries, key_rows, preferred_element_type=jnp....]
    add x17 -> x0, other arithmetic: 30.6 us -> none  [the longest x4 25.8 us: block_work(): weighted * shrink[:, :, None] + update.reshape(unit_count, query_count, -1)]
    ppermute x15 -> x0, starting transfers between devices: 13.9 us -> none  [the longest x8 6.48 us: from_partner(): return lax.ppermute(block, axis, route)]
    all_gather x1 -> x0, waiting for transfers between devices: 12.3 us -> none  [per_device(): project_incoming = lax.all_gather(normed, 'tp', axis=0, tiled=True)]
    reduce_scatter x1 -> x0, waiting for transfers between devices: 11.9 us -> none  [per_device(): lax.psum_scatter((partial_value + jnp.dot(pool_out, pool_out_weight, pref...]
    convert_element_type x20 -> x0, other arithmetic: 11.6 us -> none  [the longest x3 6.09 us: block_work(): raised.astype(jnp.bfloat16)]
  transfers between devices with their start and end apart: 17 -> 0, of which waited for: 12 -> 0; matrix products, arithmetic and copies ran while one was open for 24% -> 0% of each run, Pallas kernels for 0% -> 0%
where the time goes in v1:
time: 79.9 us; the launch traced here: 79.4 us
  Pallas kernels  77.5 us (97%)
  local copies, waits for them, and re-layouts  1.88 us (2%)
    pallas_call x1, Pallas kernels, whole_layer(): pl.pallas_call(functools.partial(layer_kernel, sp_count, members), out_sh...  77.5 us
    unnamed x1, local copies, waits for them, and re-layouts  1.88 us

profile of v1, /device:TPU:25, one launch (start us, length us, event | category | flops | bytes accessed | tf_op | source)
XLA Modules:
  0.0 79.4 jit_solution(12004678777148690811)
XLA Ops:
  0.0 77.5 %shard_map.100 = bf16[128,2048]{1,0:T(8,128)(2,1)} custom-call(bf16[128,2048]{1,0:T(8,128)(2,1)} %x_ref.1, bf16[4,128,128]{2,1,0:T(8,128)(2,1)} %pool_weight.1, f32[8]{0:T(128)} %balance.1, f32[1,256]{1,0:T(1,128)} %bitcast.1, bf16[2048,1024]{1,0:T(8,128)(2,1)} %query_hbm.1, bf16[2048,1024]{1,0:T(8,128)(2,1)} %key_hbm.1, bf16[2048,1024]{1,0:T(8,128)(2,1)} %value_hbm.1, ...), custom_call_target="tpu_custom_call" | custom-call | tf_op jit(solution)/shard_map/pallas_call | solution.py:760
  77.5 1.9 %copy.12 = bf16[128,2048]{1,0:T(8,128)(2,1)} copy(bf16[128,2048]{1,0:T(8,128)(2,1)} %shard_map.100) | data formatting | bytes 1048576

commit v2 on v1

--- a/solution.py
+++ b/solution.py
@@ -267,6 +267,7 @@
     contrast_hbm,
     pool_out_hbm,
     out_ref,
+    out_recv,
     query_w,
     key_w,
     value_w,
@@ -287,7 +288,6 @@
     rim_stage,
     pool_part,
     out_stage,
-    out_recv,
     weight_sem,
     local_sem,
     pair_send,
@@ -474,11 +474,12 @@
 
     log_scale = head_dim ** (-0.5) * math.log2(math.e)
 
-    def attend_block(step, i, seen):
+    def attend_block(step, i, blocks):
+        seen = len(blocks)
         for u in range(2):
             cols = slice(u * head_dim, (u + 1) * head_dim)
-            keys = kv[step, :seen, :, cols].reshape(seen * rows, head_dim)
-            values = kv[step, :seen, :, width:].reshape(seen * rows, width)
+            keys = jnp.concatenate([kv[step, b, :, cols] for b in blocks], axis=0)
+            values = jnp.concatenate([kv[step, b, :, width:] for b in blocks], axis=0)
             scores = lax.dot_general(
                 queries[i, :, cols], keys, (((1,), (1,)), ((), ())), preferred_element_type=f32
             )
@@ -501,24 +502,60 @@
             totals[u, i] = jnp.broadcast_to(total, totals.shape[2:])
             weighted[u, i] = update
 
+    weight = balance[tp * members + member]
+
+    def finish(i, j):
+        first = (weighted[0, i] / totals[0, i][:, :1]).astype(bf16).astype(f32)
+        second = (weighted[1, i] / totals[1, i][:, :1]).astype(bf16).astype(f32)
+        contrast = first - weight * second
+        mean_square = jnp.mean(contrast * contrast, axis=1, keepdims=True)
+        result = (contrast * lax.rsqrt(mean_square + norm_epsilon) * gain[...]).astype(bf16)
+
+        @pl.when(j > 0)
+        def _():
+            contrast_stage[j] = result
+            contrast_copy(j).start()
+
+        @pl.when(j == 0)
+        def _():
+            contrasts[member] = result
+
     def attend_own():
         for j in range(1, members):
             query_copy(j).wait_recv()
             kv_copy(0, j).wait_recv()
         for i in range(members):
-            attend_block(0, i, i + 1)
+            attend_block(0, i, list(range(i + 1)))
+
+            @pl.when(band == 0)
+            def _(i=i):
+                finish(i, flipped(member, i, members))
+
+    early = [0] + list(range(members // 2 + 1, members))
+    late = [j for j in range(1, members) if j not in early]
 
     def attend_band(step):
         @pl.when(band >= step)
         def _():
-            for j in range(1, members):
-                kv_copy(step, j).wait_recv()
-
-            def one(i, carry):
-                attend_block(step, i, members)
-                return carry
-
-            lax.fori_loop(0, members, one, 0)
+            for part in (early, late):
+                for j in part:
+                    if j > 0:
+                        kv_copy(step, j).wait_recv()
+                blocks = [flipped(member, j, members) for j in part]
+
+                def one(t, carry, part=part, blocks=blocks):
+                    j = members - 1 - t
+                    i = flipped(member, j, members)
+                    attend_block(step, i, blocks)
+                    if part is late:
+
+                        @pl.when(band == step)
+                        def _():
+                            finish(i, j)
+
+                    return carry
+
+                lax.fori_loop(0, members, one, 0)
 
     keep.wait()
     loads[0].wait()
@@ -584,29 +621,6 @@
     for step in range(max(bands - 2, 1), bands):
         attend_band(step)
 
-    weight = balance[tp * members + member]
-
-    def finish(t, carry):
-        j = members - 1 - t
-        i = flipped(member, j, members)
-        first = (weighted[0, i] / totals[0, i][:, :1]).astype(bf16).astype(f32)
-        second = (weighted[1, i] / totals[1, i][:, :1]).astype(bf16).astype(f32)
-        contrast = first - weight * second
-        mean_square = jnp.mean(contrast * contrast, axis=1, keepdims=True)
-        result = (contrast * lax.rsqrt(mean_square + norm_epsilon) * gain[...]).astype(bf16)
-
-        @pl.when(j > 0)
-        def _():
-            contrast_stage[j] = result
-            contrast_copy(j).start()
-
-        @pl.when(j == 0)
-        def _():
-            contrasts[member] = result
-
-        return carry
-
-    lax.fori_loop(0, members, finish, 0)
     loads[5].wait()
     for j in range(1, members):
         contrast_copy(j).wait_recv()
@@ -629,8 +643,6 @@
     out_copy.start()
     projected(tp, to_self)
     out_copy.wait()
-    out_ref[...] = (out_ref[...].astype(f32) + out_recv[...].astype(f32)).astype(bf16)
-
     pair_copy(0).wait_send()
     for j in range(1, members):
         query_copy(j).wait_send()
@@ -681,7 +693,6 @@
         pltpu.VMEM((reach_back + 1, pool_cols), bf16),
         pltpu.VMEM((rows, model), jnp.float32),
         pltpu.VMEM((half, model), bf16),
-        pltpu.VMEM((half, model), bf16),
         dma((6,)),
         dma,
         dma((bands,)),
@@ -757,11 +768,11 @@
         )
     vmem = pl.BlockSpec(memory_space=pltpu.VMEM)
     hbm = pl.BlockSpec(memory_space=pl.ANY)
-    return pl.pallas_call(
+    own_part, partner_part = pl.pallas_call(
         functools.partial(layer_kernel, sp_count, members),
-        out_shape=jax.ShapeDtypeStruct((half, model), jnp.bfloat16),
+        out_shape=[jax.ShapeDtypeStruct((half, model), jnp.bfloat16)] * 2,
         in_specs=[vmem, vmem, pl.BlockSpec(memory_space=pltpu.SMEM), vmem] + [hbm] * 6,
-        out_specs=vmem,
+        out_specs=[vmem, vmem],
         scratch_shapes=scratch,
         compiler_params=pltpu.CompilerParams(
             collective_id=0, has_side_effects=True, vmem_limit_bytes=vmem_most
@@ -778,6 +789,7 @@
         contrast_out_weight,
         pool_out_weight,
     )
+    return (own_part.astype(jnp.float32) + partner_part.astype(jnp.float32)).astype(jnp.bfloat16)
 
 
 def solution(mesh):

time: 79.9 us -> 80.5 us (level)
  other arithmetic: 0 us -> 2.12 us
  local copies, waits for them, and re-layouts: 1.88 us -> 0 us
    convert_element_type x0 -> x1, other arithmetic: none -> 2.12 us  [whole_layer(): (own_part.astype(jnp.float32) + partner_part.astype(jnp.float32)).astype(...]
    unnamed x1 -> x0, local copies, waits for them, and re-layouts: 1.88 us -> none
where the time goes in v2:
time: 80.5 us; the launch traced here: 80.3 us
  Pallas kernels  78.2 us (97%)
  other arithmetic  2.12 us (3%)
    pallas_call x1, Pallas kernels, whole_layer(): pl.pallas_call(functools.partial(layer_kernel, sp_count, members), out_sh...  78.2 us
    convert_element_type x1, other arithmetic, whole_layer(): (own_part.astype(jnp.float32) + partner_part.astype(jnp.float32)).astype(...  2.12 us

profile of v2, /device:TPU:25, one launch (start us, length us, event | category | flops | bytes accessed | tf_op | source)
XLA Modules:
  0.0 80.3 jit_solution(5481205150162860125)
XLA Ops:
  0.0 78.2 %shard_map.100 = (bf16[128,2048]{1,0:T(8,128)(2,1)}, bf16[128,2048]{1,0:T(8,128)(2,1)}) custom-call(bf16[128,2048]{1,0:T(8,128)(2,1)} %x_ref.1, bf16[4,128,128]{2,1,0:T(8,128)(2,1)} %pool_weight.1, f32[8]{0:T(128)} %balance.1, f32[1,256]{1,0:T(1,128)} %bitcast.1, bf16[2048,1024]{1,0:T(8,128)(2,1)} %query_hbm.1, bf16[2048,1024]{1,0:T(8,128)(2,1)} %key_hbm.1, ...), custom_call_target="tpu_custom_call" | custom-call | tf_op jit(solution)/shard_map/pallas_call | solution.py:771
  78.2 2.1 %add_convert_fusion = bf16[128,2048]{1,0:T(8,128)(2,1)} fusion(bf16[128,2048]{1,0:T(8,128)(2,1)} %get-tuple-element.8, bf16[128,2048]{1,0:T(8,128)(2,1)} %get-tuple-element.7), kind=kLoop, calls=%fused_computation | loop fusion | flops 1048576 | bytes 1572864 | tf_op jit(solution)/shard_map/convert_element_type | solution.py:792

commit v3 on v2

--- a/solution.py
+++ b/solution.py
@@ -424,7 +424,7 @@
 
     def project(step):
         def one(t, carry):
-            j = members - 1 - t
+            j = lax.rem(t + 1, members)
             head = flipped(member, j, members)
             columns = pl.ds(pl.multiple_of(head * width, width), width)
             x = rows_in[step].reshape(rows, model)
@@ -531,23 +531,22 @@
             def _(i=i):
                 finish(i, flipped(member, i, members))
 
-    early = [0] + list(range(members // 2 + 1, members))
-    late = [j for j in range(1, members) if j not in early]
+    parts = (list(range(members)),)
 
     def attend_band(step):
         @pl.when(band >= step)
         def _():
-            for part in (early, late):
+            for part in parts:
                 for j in part:
                     if j > 0:
                         kv_copy(step, j).wait_recv()
                 blocks = [flipped(member, j, members) for j in part]
 
                 def one(t, carry, part=part, blocks=blocks):
-                    j = members - 1 - t
+                    j = lax.rem(t + 1, members)
                     i = flipped(member, j, members)
                     attend_block(step, i, blocks)
-                    if part is late:
+                    if part is parts[-1]:
 
                         @pl.when(band == step)
                         def _():

time: 80.5 us -> 77.9 us (0.968)
  Pallas kernels: 78.2 us -> 75.6 us
    pallas_call x1, Pallas kernels: 78.2 us -> 75.6 us  [whole_layer(): pl.pallas_call(functools.partial(layer_kernel, sp_count, members), out_sh...]
where the time goes in v3:
time: 77.9 us; the launch traced here: 77.7 us
  Pallas kernels  75.6 us (97%)
  other arithmetic  2.12 us (3%)
    pallas_call x1, Pallas kernels, whole_layer(): pl.pallas_call(functools.partial(layer_kernel, sp_count, members), out_sh...  75.6 us
    convert_element_type x1, other arithmetic, whole_layer(): (own_part.astype(jnp.float32) + partner_part.astype(jnp.float32)).astype(...  2.12 us

profile of v3, /device:TPU:25, one launch (start us, length us, event | category | flops | bytes accessed | tf_op | source)
XLA Modules:
  0.0 77.7 jit_solution(8664566973585230077)
XLA Ops:
  0.0 75.6 %shard_map.100 = (bf16[128,2048]{1,0:T(8,128)(2,1)}, bf16[128,2048]{1,0:T(8,128)(2,1)}) custom-call(bf16[128,2048]{1,0:T(8,128)(2,1)} %x_ref.1, bf16[4,128,128]{2,1,0:T(8,128)(2,1)} %pool_weight.1, f32[8]{0:T(128)} %balance.1, f32[1,256]{1,0:T(1,128)} %bitcast.1, bf16[2048,1024]{1,0:T(8,128)(2,1)} %query_hbm.1, bf16[2048,1024]{1,0:T(8,128)(2,1)} %key_hbm.1, ...), custom_call_target="tpu_custom_call" | custom-call | tf_op jit(solution)/shard_map/pallas_call | solution.py:770
  75.6 2.1 %add_convert_fusion = bf16[128,2048]{1,0:T(8,128)(2,1)} fusion(bf16[128,2048]{1,0:T(8,128)(2,1)} %get-tuple-element.8, bf16[128,2048]{1,0:T(8,128)(2,1)} %get-tuple-element.7), kind=kLoop, calls=%fused_computation | loop fusion | flops 1048576 | bytes 1572864 | tf_op jit(solution)/shard_map/convert_element_type | solution.py:791
